TPU v7x, 32 devices: a whole 2x2x4 slice. The times are simulated.
32 devices in a mesh: fs: 8 (over z, y), tp: 4 (over x, core).
Axes of the slice: x: 2, y: 2, z: 4, core: 2. Of those that a mesh axis runs over, the one named last changes fastest.
Arguments:
- tokens: bfloat16 [3072, 2048], P('fs'), may hold values from -6 to 6
- norm_gain: float32 [2048], replicated, may hold values from 0.1 to 1.9
- w_gate: bfloat16 [2048, 4096], P('fs', 'tp'), may hold values from -0.125 to 0.125
- w_up: bfloat16 [2048, 4096], P('fs', 'tp'), may hold values from -0.125 to 0.125
- w_down: bfloat16 [4096, 2048], P('tp', 'fs'), may hold values from -0.09375 to 0.09375
- cotangent: bfloat16 [3072, 2048], P('fs'), may hold values from -6 to 6
Outputs:
- grad_tokens: bfloat16 [3072, 2048], P('fs')
- grad_down: float32 [4096, 2048], P('tp', 'fs')
- down_norms: float32 [4096], P('tp')
All inputs are finite; a program needn't handle non-finite values.
Results may differ from a plain program's by a relative error of at most 0.018.
Values may be sent and summed in bfloat16 or wider, within the bound.
A program may use at most 64 MiB of HBM per device.

v0:
```python
import jax
import jax.numpy as jnp
from jax import lax
from jax.sharding import PartitionSpec as P

EPS = 1e-06


def shards(tokens, norm_gain, w_gate, w_up, w_down, cotangent):
    xf = tokens.astype(jnp.float32)
    inv = lax.rsqrt(jnp.mean(xf * xf, axis=-1, keepdims=True) + EPS)
    scaled = xf * inv
    normed = (scaled * norm_gain).astype(jnp.bfloat16)
    full_gate, full_up = (
        lax.all_gather(w_gate, "fs", axis=0, tiled=True),
        lax.all_gather(w_up, "fs", axis=0, tiled=True),
    )
    gate = jnp.dot(normed, full_gate, preferred_element_type=jnp.float32)
    up = jnp.dot(normed, full_up, preferred_element_type=jnp.float32)
    full_down = lax.all_gather(w_down, "fs", axis=1, tiled=True)
    d_hidden = 0.5 * lax.dot_general(
        cotangent, full_down, (((1,), (1,)), ((), ())), preferred_element_type=jnp.float32
    )
    sig = jax.nn.sigmoid(gate)
    act = gate * sig
    hidden = (act * up).astype(jnp.bfloat16)
    share = lax.psum_scatter(
        0.5
        * lax.dot_general(
            cotangent, hidden, (((0,), (0,)), ((), ())), preferred_element_type=jnp.float32
        ),
        "fs",
        scatter_dimension=0,
        tiled=True,
    )
    grad_down = share.T
    down_norms = lax.psum(jnp.sum(share * share, axis=0), "fs")
    d_gate = (d_hidden * up * sig * (1.0 + gate * (1.0 - sig))).astype(jnp.bfloat16)
    d_up = (d_hidden * act).astype(jnp.bfloat16)
    part = lax.dot_general(
        d_gate, full_gate, (((1,), (1,)), ((), ())), preferred_element_type=jnp.float32
    )
    part = part + lax.dot_general(
        d_up, full_up, (((1,), (1,)), ((), ())), preferred_element_type=jnp.float32
    )
    d_normed = lax.psum(part.astype(jnp.bfloat16), "tp").astype(jnp.float32)
    d_scaled = d_normed * norm_gain
    inner = jnp.mean(d_scaled * scaled, axis=-1, keepdims=True)
    grad_tokens = (inv * (d_scaled - scaled * inner)).astype(jnp.bfloat16)
    return (grad_tokens, grad_down, down_norms)


def solution(mesh):
    in_specs = (P("fs", None), P(), P("fs", "tp"), P("fs", "tp"), P("tp", "fs"), P("fs", None))
    out_specs = (P("fs", None), P("tp", "fs"), P("tp"))
    return jax.shard_map(shards, mesh=mesh, in_specs=in_specs, out_specs=out_specs, check_vma=False)
```

profile of v0, /device:TPU:0, one launch (start us, length us, event | category | flops | bytes accessed | tf_op | source)
XLA Modules:
  0.0 465.4 jit_solution(9571083893437479474)
XLA Ops:
  7.2 0.0 copy-start
  7.2 0.0 all-gather.8.cloned.1.call-start
  7.2 0.7 all-gather.8.cloned.1.call-update
  7.9 0.0 all-gather.6.cloned.1.call-start
  8.0 0.7 all-gather.6.cloned.1.call-update
  8.7 0.0 all-gather.4.cloned.1.call-start
  8.7 0.7 all-gather.4.cloned.1.call-update
  9.4 0.0 all-reduce.2.cloned.1.call-start
  9.5 1.8 fusion.8
  11.3 74.4 %all-gather.8.cloned.1.call-done = bf16[2048,1024]{1,0:T(8,128)(2,1)} async-done(((bf16[256,1024]{1,0:T(8,128)(2,1)}), bf16[2048,1024]{1,0:T(8,128)(2,1)}) %all-gather.8.cloned.1.call-update) | async-done | bytes 4194320 | tf_op jit(solution)/shard_map/all_gather | solution.py:15
  85.7 5.2 %fusion.12 = f32[384,1024]{1,0:T(8,128)} fusion(bf16[2048,1024]{1,0:T(8,128)(2,1)} %all-gather.8.cloned.1.call-done, bf16[384,2048]{1,0:T(8,128)(2,1)S(1)} %copy-done.1, f32[2048]{0:T(1024)S(1)} %copy-done.3, f32[384]{0:T(512)S(1)} %add_rsqrt_fusion), kind=kOutput, calls=%fused_computation.23 | convolution fusion | flops 1613758464 | bytes 7349760 | tf_op jit(solution)/shard_map/dot_general | solution.py:18
  90.9 68.3 %all-gather.6.cloned.1.call-done = bf16[2048,1024]{1,0:T(8,128)(2,1)} async-done(((bf16[256,1024]{1,0:T(8,128)(2,1)}), bf16[2048,1024]{1,0:T(8,128)(2,1)}) %all-gather.6.cloned.1.call-update) | async-done | bytes 4194320 | tf_op jit(solution)/shard_map/all_gather | solution.py:16
  159.2 5.2 %fusion.14 = f32[384,1024]{1,0:T(8,128)} fusion(bf16[2048,1024]{1,0:T(8,128)(2,1)} %all-gather.6.cloned.1.call-done, bf16[384,2048]{1,0:T(8,128)(2,1)S(1)} %copy-done.1, f32[2048]{0:T(1024)S(1)} %copy-done.3, f32[384]{0:T(512)S(1)} %add_rsqrt_fusion), kind=kOutput, calls=%fused_computation.24 | convolution fusion | flops 1613758464 | bytes 7349760 | tf_op jit(solution)/shard_map/dot_general | solution.py:19
  164.4 70.0 %all-gather.4.cloned.1.call-done = bf16[1024,2048]{1,0:T(8,128)(2,1)} async-done(((bf16[1024,256]{1,0:T(8,128)(2,1)}), bf16[1024,2048]{1,0:T(8,128)(2,1)}) %all-gather.4.cloned.1.call-update) | async-done | bytes 4194320 | tf_op jit(solution)/shard_map/all_gather | solution.py:20
  234.4 0.0 copy-done
  234.4 4.2 convolution_multiply_fusion
  238.6 0.0 copy-done.4
  238.6 0.0 copy-done.6
  238.6 0.2 copy-done.7
  238.8 2.3 fusion.10
  241.1 0.0 copy-done.5
  241.1 3.0 add_convert_fusion
  244.1 0.0 all-reduce.2.cloned.1.call-update
  244.1 0.2 reduce-scatter.2.cloned.1.call-start
  244.4 7.5 %multiply_bitcast_fusion = f32[2048,1024]{0,1:T(8,128)} fusion(bf16[384,2048]{1,0:T(8,128)(2,1)S(1)} %copy-done, f32[384,1024]{1,0:T(8,128)} %fusion.14, f32[384,1024]{1,0:T(8,128)} %fusion.12), kind=kOutput, calls=%fused_computation | convolution fusion | flops 1615069184 | bytes 13107200 | tf_op jit(solution)/shard_map/dot_general | solution.py:29
  251.9 0.0 reduce-scatter.2.cloned.1.call-update
  251.9 33.4 %all-reduce.2.cloned.1.call-done = bf16[384,2048]{1,0:T(8,128)(2,1)} async-done(((bf16[384,2048]{1,0:T(8,128)(2,1)}), bf16[384,2048]{1,0:T(8,128)(2,1)}) %all-reduce.2.cloned.1.call-update) | async-done | bytes 1572880 | tf_op jit(solution)/shard_map/psum | solution.py:46
  285.3 2.3 fusion.4
  287.6 2.0 fusion.7
  289.6 147.7 %reduce-scatter.2.cloned.1.call-done = f32[256,1024]{0,1:T(8,128)} async-done(((f32[2048,1024]{0,1:T(8,128)}), f32[256,1024]{0,1:T(8,128)}) %reduce-scatter.2.cloned.1.call-update) | async-done | bytes 1048592 | tf_op jit(solution)/shard_map/reduce_scatter | solution.py:27
  437.3 1.4 multiply_reduce_fusion
  438.8 20.1 %psum.15 = f32[1024]{0:T(1024)} all-reduce(f32[1024]{0:T(1024)S(1)} %multiply_reduce_fusion), channel_id=1, replica_groups=mesh['fs'=8,'tp'=4] {'fs'}, use_global_device_ids=true, to_apply=%region_5.0 | all-reduce | flops 1024 | bytes 8192 | tf_op jit(solution)/shard_map/psum | solution.py:37
  (12 shorter events, 0.0 us)
Async XLA Ops:
  7.2 227.3 %copy-start = (bf16[384,2048]{1,0:T(8,128)(2,1)S(1)}, bf16[384,2048]{1,0:T(8,128)(2,1)}, u32[]{:S(2)}) copy-start(bf16[384,2048]{1,0:T(8,128)(2,1)} %param.11) | copy-start | bytes 4718596
  7.2 78.5 %copy-start.1 = (bf16[384,2048]{1,0:T(8,128)(2,1)S(1)}, bf16[384,2048]{1,0:T(8,128)(2,1)}, u32[]{:S(2)}) copy-start(bf16[384,2048]{1,0:T(8,128)(2,1)} %param.6) | copy-start | bytes 4718596
  7.2 78.5 %copy-start.3 = (f32[2048]{0:T(1024)S(1)}, f32[2048]{0:T(1024)}, u32[]{:S(2)}) copy-start(f32[2048]{0:T(1024)} %param.7) | copy-start | bytes 24580
  7.2 78.5 %all-gather.8.cloned.1.call-start = ((), (), s32[]{:S(2)}) async-start(), calls=%async_computation.3 | async-start | bytes 4718592 | tf_op jit(solution)/shard_map/all_gather | solution.py:15
  7.9 151.2 %all-gather.6.cloned.1.call-start = ((), (), s32[]{:S(2)}) async-start(), calls=%async_computation.2 | async-start | bytes 4718592 | tf_op jit(solution)/shard_map/all_gather | solution.py:16
  8.7 225.7 %all-gather.4.cloned.1.call-start = ((), (), s32[]{:S(2)}) async-start(), calls=%async_computation.1 | async-start | bytes 4718592 | tf_op jit(solution)/shard_map/all_gather | solution.py:20
  9.4 275.9 %all-reduce.2.cloned.1.call-start = ((), (), s32[]{:S(2)}) async-start(), calls=%async_computation.4 | async-start | bytes 3145728 | tf_op jit(solution)/shard_map/psum | solution.py:46
  234.4 4.2 copy-start.4
  234.4 4.2 copy-start.6
  234.4 4.4 copy-start.7
  238.8 2.3 copy-start.5
  244.1 193.2 %reduce-scatter.2.cloned.1.call-start = ((), (), s32[]{:S(2)}) async-start(), calls=%async_computation.5 | async-start | bytes 9437184 | tf_op jit(solution)/shard_map/reduce_scatter | solution.py:27
  285.3 2.3 copy-start.2
Sparse Core Ops, SparseCore 0:
  10.1 75.5 all-gather.7
  87.8 71.3 all-gather.5
  161.2 73.1 all-gather.3
  244.2 41.0 all-reduce.1
  289.4 147.9 reduce-scatter.1
where the time goes:
time: 466 us; the launch traced here: 465 us
  waiting for transfers between devices  396 us (85%)
  matrix products  27.3 us (6%)
  blocking collectives  20.1 us (4%)
  between operations  13.9 us (3%)
  other arithmetic  7.55 us (2%)
    reduce_scatter x1, waiting for transfers between devices, shards(): lax.psum_scatter(0.5 * lax.dot_general(cotangent, hidden, (((0,), (0,)),...  148 us
    all_gather x1, waiting for transfers between devices, shards(): lax.all_gather(w_gate, 'fs', axis=0, tiled=True)  74.4 us
    all_gather x1, waiting for transfers between devices, shards(): full_down = lax.all_gather(w_down, 'fs', axis=1, tiled=True)  70 us
    all_gather x1, waiting for transfers between devices, shards(): lax.all_gather(w_up, 'fs', axis=0, tiled=True)  68.3 us
    psum x1, waiting for transfers between devices, shards(): d_normed = lax.psum(part.astype(jnp.bfloat16), 'tp').astype(jnp.float32)  33.4 us
    psum x1, blocking collectives, shards(): down_norms = lax.psum(jnp.sum(share * share, axis=0), 'fs')  20.1 us
  transfers between devices with their start and end apart: 5, of which 5 were waited for; matrix products, arithmetic and copies ran while one was open for 5% of the time, Pallas kernels for 0%

commit v1 on v0

--- a/solution.py
+++ b/solution.py
@@ -17,7 +17,12 @@
     )
     gate = jnp.dot(normed, full_gate, preferred_element_type=jnp.float32)
     up = jnp.dot(normed, full_up, preferred_element_type=jnp.float32)
-    full_down = lax.all_gather(w_down, "fs", axis=1, tiled=True)
+    ring = [w_down]
+    for hop in range(7):
+        ring.append(lax.ppermute(ring[-1], "fs", [(dev, (dev + 1) % 8) for dev in range(8)]))
+    full_down = jnp.roll(
+        jnp.concatenate(ring[::-1], axis=1), (lax.axis_index("fs") + 1) * ring[0].shape[1], axis=1
+    )
     d_hidden = 0.5 * lax.dot_general(
         cotangent, full_down, (((1,), (1,)), ((), ())), preferred_element_type=jnp.float32
     )

time: 466 us -> 440 us (0.944)
  waiting for transfers between devices: 396 us -> 359 us
  local copies, waits for them, and re-layouts: 0.24 us -> 7.33 us
    ppermute x0 -> x7, waiting for transfers between devices: none -> 153 us  [shards(): lax.ppermute(ring[-1], 'fs', [(dev, (dev + 1) % 8) for dev in range(8)])]
    all_gather x1, waiting for transfers between devices: 74.4 us -> 0.01 us  [shards(): lax.all_gather(w_gate, 'fs', axis=0, tiled=True)]
    all_gather x1 -> x0, waiting for transfers between devices: 70 us -> none  [shards(): full_down = lax.all_gather(w_down, 'fs', axis=1, tiled=True)]
    all_gather x1, waiting for transfers between devices: 68.3 us -> 23.3 us  [shards(): lax.all_gather(w_up, 'fs', axis=0, tiled=True)]
    unnamed x16 -> x43, local copies, waits for them, and re-layouts: 0.24 us -> 7.27 us
  transfers between devices with their start and end apart: 5 -> 11, of which waited for: 5 -> 10; matrix products, arithmetic and copies ran while one was open for 5% -> 6% of each run, Pallas kernels for 0% -> 0%
where the time goes in v1:
time: 440 us; the launch traced here: 439 us
  waiting for transfers between devices  359 us (82%)
  matrix products  26.9 us (6%)
  blocking collectives  20.1 us (5%)
  between operations  14 us (3%)
  other arithmetic  7.61 us (2%)
  local copies, waits for them, and re-layouts  7.33 us (2%)
    ppermute x7, waiting for transfers between devices, shards(): lax.ppermute(ring[-1], 'fs', [(dev, (dev + 1) % 8) for dev in range(8)])  153 us
    reduce_scatter x1, waiting for transfers between devices, shards(): lax.psum_scatter(0.5 * lax.dot_general(cotangent, hidden, (((0,), (0,)),...  148 us
    psum x1, waiting for transfers between devices, shards(): d_normed = lax.psum(part.astype(jnp.bfloat16), 'tp').astype(jnp.float32)  33.8 us
    all_gather x1, waiting for transfers between devices, shards(): lax.all_gather(w_up, 'fs', axis=0, tiled=True)  23.3 us
    psum x1, blocking collectives, shards(): down_norms = lax.psum(jnp.sum(share * share, axis=0), 'fs')  20.1 us
  transfers between devices with their start and end apart: 11, of which 10 were waited for; matrix products, arithmetic and copies ran while one was open for 6% of the time, Pallas kernels for 0%

profile of v1, /device:TPU:0, one launch (start us, length us, event | category | flops | bytes accessed | tf_op | source)
XLA Modules:
  0.0 439.3 jit_solution(16170239079108986037)
XLA Ops:
  7.2 0.7 all-gather.5.cloned.1.call-update
  8.0 0.7 all-gather.3.cloned.1.call-update
  8.7 3.0 collective-permute-start
  11.8 15.7 %collective-permute-done = bf16[1024,256]{1,0:T(8,128)(2,1)S(1)} collective-permute-done((bf16[1024,256]{1,0:T(8,128)(2,1)}, bf16[1024,256]{1,0:T(8,128)(2,1)S(1)}, u32[]{:S(2)}, u32[]{:S(2)}) %collective-permute-start) | collective-permute-done | bytes 524320 | tf_op jit(solution)/shard_map/ppermute | solution.py:22
  27.5 1.0 collective-permute-start.1
  28.4 26.6 %collective-permute-done.1 = bf16[1024,256]{1,0:T(8,128)(2,1)S(1)} collective-permute-done((bf16[1024,256]{1,0:T(8,128)(2,1)S(1)}, bf16[1024,256]{1,0:T(8,128)(2,1)S(1)}, u32[]{:S(2)}, u32[]{:S(2)}) %collective-permute-start.1) | collective-permute-done | bytes 524320 | tf_op jit(solution)/shard_map/ppermute | solution.py:22
  55.1 25.6 %collective-permute-done.2 = bf16[1024,256]{1,0:T(8,128)(2,1)S(1)} collective-permute-done((bf16[1024,256]{1,0:T(8,128)(2,1)S(1)}, bf16[1024,256]{1,0:T(8,128)(2,1)S(1)}, u32[]{:S(2)}, u32[]{:S(2)}) %collective-permute-start.2) | collective-permute-done | bytes 524320 | tf_op jit(solution)/shard_map/ppermute | solution.py:22
  80.7 26.7 %collective-permute-done.3 = bf16[1024,256]{1,0:T(8,128)(2,1)S(1)} collective-permute-done((bf16[1024,256]{1,0:T(8,128)(2,1)S(1)}, bf16[1024,256]{1,0:T(8,128)(2,1)S(1)}, u32[]{:S(2)}, u32[]{:S(2)}) %collective-permute-start.3) | collective-permute-done | bytes 524320 | tf_op jit(solution)/shard_map/ppermute | solution.py:22
  107.3 0.8 copy-done.4
  108.1 18.2 %collective-permute-done.4 = bf16[1024,256]{1,0:T(8,128)(2,1)S(1)} collective-permute-done((bf16[1024,256]{1,0:T(8,128)(2,1)S(1)}, bf16[1024,256]{1,0:T(8,128)(2,1)S(1)}, u32[]{:S(2)}, u32[]{:S(2)}) %collective-permute-start.4) | collective-permute-done | bytes 524320 | tf_op jit(solution)/shard_map/ppermute | solution.py:22
  126.3 0.8 copy-done.6
  127.1 24.4 %collective-permute-done.5 = bf16[1024,256]{1,0:T(8,128)(2,1)} collective-permute-done((bf16[1024,256]{1,0:T(8,128)(2,1)S(1)}, bf16[1024,256]{1,0:T(8,128)(2,1)}, u32[]{:S(2)}, u32[]{:S(2)}) %collective-permute-start.5) | collective-permute-done | bytes 524320 | tf_op jit(solution)/shard_map/ppermute | solution.py:22
  151.4 1.9 fusion.10
  153.3 15.5 %collective-permute-done.6 = bf16[1024,256]{1,0:T(8,128)(2,1)} collective-permute-done((bf16[1024,256]{1,0:T(8,128)(2,1)}, bf16[1024,256]{1,0:T(8,128)(2,1)}, u32[]{:S(2)}, u32[]{:S(2)}) %collective-permute-start.6) | collective-permute-done | bytes 524320 | tf_op jit(solution)/shard_map/ppermute | solution.py:22
  168.9 1.1 constant_dynamic-update-slice_fusion.15
  170.0 1.2 constant_dynamic-update-slice_fusion.14
  171.6 1.1 constant_dynamic-update-slice_fusion.7
  172.7 1.1 constant_dynamic-update-slice_fusion.6
  174.3 3.5 fusion.16
  177.8 5.8 %fusion.23 = f32[384,1024]{0,1:T(8,128)} fusion(bf16[2048,1024]{1,0:T(8,128)(2,1)} %all-gather.5.cloned.1.call-done, bf16[384,2048]{1,0:T(8,128)(2,1)S(1)} %copy-done.1, f32[2048]{0:T(1024)S(1)} %copy-done.8, f32[384]{0:T(512)S(1)} %add_rsqrt_fusion), kind=kOutput, calls=%fused_computation.29 | convolution fusion | flops 1613758464 | bytes 7349760 | tf_op jit(solution)/shard_map/dot_general | solution.py:18
  183.7 23.3 %all-gather.3.cloned.1.call-done = bf16[2048,1024]{1,0:T(8,128)(2,1)} async-done(((bf16[256,1024]{1,0:T(8,128)(2,1)}), bf16[2048,1024]{1,0:T(8,128)(2,1)}) %all-gather.3.cloned.1.call-update) | async-done | bytes 4194320 | tf_op jit(solution)/shard_map/all_gather | solution.py:16
  207.0 4.8 %fusion.25 = f32[384,1024]{0,1:T(8,128)S(1)} fusion(bf16[2048,1024]{1,0:T(8,128)(2,1)} %all-gather.3.cloned.1.call-done, bf16[384,2048]{1,0:T(8,128)(2,1)S(1)} %copy-done.1, f32[2048]{0:T(1024)S(1)} %copy-done.8, f32[384]{0:T(512)S(1)} %add_rsqrt_fusion), kind=kOutput, calls=%fused_computation.30 | convolution fusion | flops 1613758464 | bytes 7349760 | tf_op jit(solution)/shard_map/dot_general | solution.py:19
  211.8 2.3 fusion.20
  214.1 0.4 copy-done.10
  214.6 3.1 add_convert_fusion
  217.9 7.5 %multiply_bitcast_fusion = f32[2048,1024]{0,1:T(8,128)} fusion(bf16[384,2048]{1,0:T(8,128)(2,1)S(1)} %copy-done, f32[384,1024]{0,1:T(8,128)} %copy-done.12, f32[384,1024]{0,1:T(8,128)} %fusion.23), kind=kOutput, calls=%fused_computation | convolution fusion | flops 1615069184 | bytes 13107200 | tf_op jit(solution)/shard_map/dot_general | solution.py:34
  225.4 33.8 %all-reduce.2.cloned.1.call-done = bf16[384,2048]{1,0:T(8,128)(2,1)} async-done(((bf16[384,2048]{1,0:T(8,128)(2,1)}), bf16[384,2048]{1,0:T(8,128)(2,1)}) %all-reduce.2.cloned.1.call-update) | async-done | bytes 1572880 | tf_op jit(solution)/shard_map/psum | solution.py:51
  259.2 2.3 fusion.6
  261.5 2.0 fusion.9
  263.5 147.7 %reduce-scatter.2.cloned.1.call-done = f32[256,1024]{0,1:T(8,128)} async-done(((f32[2048,1024]{0,1:T(8,128)}), f32[256,1024]{0,1:T(8,128)}) %reduce-scatter.2.cloned.1.call-update) | async-done | bytes 1048592 | tf_op jit(solution)/shard_map/reduce_scatter | solution.py:32
  411.2 1.4 multiply_reduce_fusion
  412.7 20.1 %psum.15 = f32[1024]{0:T(1024)} all-reduce(f32[1024]{0:T(1024)S(1)} %multiply_reduce_fusion), channel_id=1, replica_groups=mesh['fs'=8,'tp'=4] {'fs'}, use_global_device_ids=true, to_apply=%region_5.6 | all-reduce | flops 1024 | bytes 8192 | tf_op jit(solution)/shard_map/psum | solution.py:42
  (51 shorter events, 1.2 us)
Async XLA Ops:
  7.2 167.1 %copy-start = (bf16[384,2048]{1,0:T(8,128)(2,1)S(1)}, bf16[384,2048]{1,0:T(8,128)(2,1)}, u32[]{:S(2)}) copy-start(bf16[384,2048]{1,0:T(8,128)(2,1)} %param.11) | copy-start | bytes 4718596
  7.2 170.6 %all-gather.5.cloned.1.call-start = ((), (), s32[]{:S(2)}) async-start(), calls=%async_computation.2 | async-start | bytes 4718592 | tf_op jit(solution)/shard_map/all_gather | solution.py:15
  7.9 199.1 %all-gather.3.cloned.1.call-start = ((), (), s32[]{:S(2)}) async-start(), calls=%async_computation.1 | async-start | bytes 4718592 | tf_op jit(solution)/shard_map/all_gather | solution.py:16
  8.7 250.5 %all-reduce.2.cloned.1.call-start = ((), (), s32[]{:S(2)}) async-start(), calls=%async_computation.3 | async-start | bytes 3145728 | tf_op jit(solution)/shard_map/psum | solution.py:51
  8.7 18.8 %collective-permute-start = (bf16[1024,256]{1,0:T(8,128)(2,1)}, bf16[1024,256]{1,0:T(8,128)(2,1)S(1)}, u32[]{:S(2)}, u32[]{:S(2)}) collective-permute-start(bf16[1024,256]{1,0:T(8,128)(2,1)} %param.10), channel_id=1, source_target_pairs={{0,4},{4,8},{8,12},{12,16},{16,20},{20,24},{24,28},{28,0},{1,5},{5... | collective-permute-start | bytes 1572872 | tf_op jit(solution)/shard_map/ppermute | solution.py:22
  27.5 27.6 %collective-permute-start.1 = (bf16[1024,256]{1,0:T(8,128)(2,1)S(1)}, bf16[1024,256]{1,0:T(8,128)(2,1)S(1)}, u32[]{:S(2)}, u32[]{:S(2)}) collective-permute-start(bf16[1024,256]{1,0:T(8,128)(2,1)S(1)} %collective-permute-done), channel_id=1, source_target_pairs={{0,4},{4,8},{8,12},{12,16},{16,20},{20,24},{24,28},{28,0},{1,5},{5... | collective-permute-start | bytes 1572872 | tf_op jit(solution)/shard_map/ppermute | solution.py:22
  55.1 25.6 %collective-permute-start.2 = (bf16[1024,256]{1,0:T(8,128)(2,1)S(1)}, bf16[1024,256]{1,0:T(8,128)(2,1)S(1)}, u32[]{:S(2)}, u32[]{:S(2)}) collective-permute-start(bf16[1024,256]{1,0:T(8,128)(2,1)S(1)} %collective-permute-done.1), channel_id=1, source_target_pairs={{0,4},{4,8},{8,12},{12,16},{16,20},{20,24},{24,28},{28,0},{1,5},{5... | collective-permute-start | bytes 1572872 | tf_op jit(solution)/shard_map/ppermute | solution.py:22
  80.7 26.7 %collective-permute-start.3 = (bf16[1024,256]{1,0:T(8,128)(2,1)S(1)}, bf16[1024,256]{1,0:T(8,128)(2,1)S(1)}, u32[]{:S(2)}, u32[]{:S(2)}) collective-permute-start(bf16[1024,256]{1,0:T(8,128)(2,1)S(1)} %collective-permute-done.2), channel_id=1, source_target_pairs={{0,4},{4,8},{8,12},{12,16},{16,20},{20,24},{24,28},{28,0},{1,5},{5... | collective-permute-start | bytes 1572872 | tf_op jit(solution)/shard_map/ppermute | solution.py:22
  107.3 0.8 copy-start.4
  108.1 18.2 %collective-permute-start.4 = (bf16[1024,256]{1,0:T(8,128)(2,1)S(1)}, bf16[1024,256]{1,0:T(8,128)(2,1)S(1)}, u32[]{:S(2)}, u32[]{:S(2)}) collective-permute-start(bf16[1024,256]{1,0:T(8,128)(2,1)S(1)} %collective-permute-done.3), channel_id=1, source_target_pairs={{0,4},{4,8},{8,12},{12,16},{16,20},{20,24},{24,28},{28,0},{1,5},{5... | collective-permute-start | bytes 1572872 | tf_op jit(solution)/shard_map/ppermute | solution.py:22
  126.3 0.8 copy-start.6
  127.1 24.4 %collective-permute-start.5 = (bf16[1024,256]{1,0:T(8,128)(2,1)S(1)}, bf16[1024,256]{1,0:T(8,128)(2,1)}, u32[]{:S(2)}, u32[]{:S(2)}) collective-permute-start(bf16[1024,256]{1,0:T(8,128)(2,1)S(1)} %collective-permute-done.4), channel_id=1, source_target_pairs={{0,4},{4,8},{8,12},{12,16},{16,20},{20,24},{24,28},{28,0},{1,5},{5... | collective-permute-start | bytes 1572872 | tf_op jit(solution)/shard_map/ppermute | solution.py:22
  151.4 17.4 %collective-permute-start.6 = (bf16[1024,256]{1,0:T(8,128)(2,1)}, bf16[1024,256]{1,0:T(8,128)(2,1)}, u32[]{:S(2)}, u32[]{:S(2)}) collective-permute-start(bf16[1024,256]{1,0:T(8,128)(2,1)} %collective-permute-done.5), channel_id=1, source_target_pairs={{0,4},{4,8},{8,12},{12,16},{16,20},{20,24},{24,28},{28,0},{1,5},{5... | collective-permute-start | bytes 1572872 | tf_op jit(solution)/shard_map/ppermute | solution.py:22
  151.4 19.7 %copy-start.7 = (bf16[1024,256]{1,0:T(8,128)(2,1)S(1)}, bf16[1024,256]{1,0:T(8,128)(2,1)}, u32[]{:S(2)}) copy-start(bf16[1024,256]{1,0:T(8,128)(2,1)} %copy-done.6) | copy-start | bytes 1572868
  151.4 19.8 %copy-start.5 = (bf16[1024,256]{1,0:T(8,128)(2,1)S(1)}, bf16[1024,256]{1,0:T(8,128)(2,1)}, u32[]{:S(2)}) copy-start(bf16[1024,256]{1,0:T(8,128)(2,1)} %copy-done.4) | copy-start | bytes 1572868
  170.0 1.6 copy-start.3
  174.3 3.5 copy-start.1
  174.3 3.5 copy-start.8
  207.0 4.8 %copy-start.9 = (bf16[2048,1024]{1,0:T(8,128)(2,1)S(1)}, bf16[2048,1024]{1,0:T(8,128)(2,1)}, u32[]{:S(2)}) copy-start(bf16[2048,1024]{1,0:T(8,128)(2,1)} %all-gather.5.cloned.1.call-done) | copy-start | bytes 12582916
  207.0 4.8 %copy-start.11 = (f32[384,1024]{0,1:T(8,128)S(1)}, f32[384,1024]{0,1:T(8,128)}, u32[]{:S(2)}) copy-start(f32[384,1024]{0,1:T(8,128)} %fusion.23) | copy-start | bytes 4718596
  207.0 4.8 %copy-start.13 = (f32[1024,384]{1,0:T(8,128)S(1)}, f32[1024,384]{1,0:T(8,128)}, u32[]{:S(2)}) copy-start(f32[1024,384]{1,0:T(8,128)} %fusion.16) | copy-start | bytes 4718596
  211.8 2.3 copy-start.12
  211.8 2.8 copy-start.10
  217.6 193.6 %reduce-scatter.2.cloned.1.call-start = ((), (), s32[]{:S(2)}) async-start(), calls=%async_computation.4 | async-start | bytes 9437184 | tf_op jit(solution)/shard_map/reduce_scatter | solution.py:32
  259.2 2.3 copy-start.2
Sparse Core Ops, SparseCore 0:
  10.1 104.3 all-gather.4
  116.6 90.3 all-gather.2
  217.8 41.3 all-reduce.1
  263.3 147.9 reduce-scatter.1
